TPU v7x, 32 devices: a whole 2x2x4 slice. The times are simulated.
32 devices in a mesh: sp: 16 (over z, x, core), tp: 2 (over y).
Axes of the slice: x: 2, y: 2, z: 4, core: 2. Of those that a mesh axis runs over, the one named last changes fastest.
Arguments:
- residual: bfloat16 [4096, 2048], P(('sp', 'tp')), may hold values from -6 to 6
- query_vectors: bfloat16 [4096, 512], P('sp', 'tp'), may hold values from -6 to 6
- key_vectors: bfloat16 [4096, 512], P('sp', 'tp'), may hold values from -6 to 6
- value_vectors: bfloat16 [4096, 512], P('sp', 'tp'), may hold values from -6 to 6
- in_gate: float32 [8, 4096], P('tp', 'sp'), may hold values from -9 to 190
- forget_gate: float32 [8, 4096], P('tp', 'sp'), may hold values from -1 to 12
- documents: int32 [4096], P('sp'), may hold values from 0 to 3, never falling along the last dimension, each value on 1 to 2048 neighbouring positions
- w_out: bfloat16 [512, 2048], P('tp'), may hold values from -0.25 to 0.25
- norm_gain: bfloat16 [2048], replicated, may hold values from 0.099609375 to 1.8984375
- w_up: bfloat16 [2048, 8192], P('sp', 'tp'), may hold values from -0.125 to 0.125
- w_down: bfloat16 [8192, 2048], P('tp', 'sp'), may hold values from -0.0625 to 0.0625
Outputs:
- layer_out: bfloat16 [4096, 2048], P(('sp', 'tp'))
Inputs may be any that keep to these rules, and one draw needn't show every extreme that they name: `documents`: document numbers never fall along the positions; every document has 1 to 2048 positions.
All inputs are finite; a program needn't handle non-finite values.
Results may differ from a plain program's by a relative error of at most 0.015.
Values may be sent and summed in bfloat16 or wider, within the bound.
A program may use at most 128 MiB of HBM per device.

v0:
```python
import jax
import jax.numpy as jnp
from jax import lax
from jax.sharding import PartitionSpec as P

SPAN = 128


very_negative = -1e30
epsilon = 1e-06


def carried_in(value, axis, combine, identity):
    length, here = (lax.axis_size(axis), lax.axis_index(axis))
    everything = jax.tree.map(lambda part: lax.all_gather(part, axis), value)
    start = jax.tree.map(
        lambda part, zero: jnp.broadcast_to(jnp.asarray(zero, part.dtype), part.shape),
        value,
        identity,
    )

    def lap(k, before):
        reached = k < here
        new = combine(before, jax.tree.map(lambda part: part[k], everything))
        return jax.tree.map(lambda a, b: jnp.where(reached, a, b), new, before)

    return lax.fori_loop(0, length, lap, start)


def identity_state(head_count, head_dim):
    return (
        jnp.zeros((head_count, head_dim, head_dim), jnp.float32),
        jnp.zeros((head_count, head_dim), jnp.float32),
        jnp.full((head_count,), very_negative, jnp.float32),
        jnp.zeros((head_count,), jnp.float32),
        jnp.array(-1.0, jnp.float32),
        jnp.array(-1.0, jnp.float32),
    )


def combine(earlier, later):
    memory_one, normal_one, top_one, decay_one, first_one, last_one = earlier
    memory_two, normal_two, top_two, decay_two, first_two, last_two = later
    later_empty = first_two < 0.0
    earlier_empty = first_one < 0.0
    keep = later_empty | (first_two == last_two) & (first_two == last_one)
    decay_step = jnp.where(later_empty, 0.0, decay_two)
    top_new = jnp.where(keep, jnp.maximum(decay_step + top_one, top_two), top_two)
    scale_old = jnp.where(keep, jnp.exp(decay_step + top_one - top_new), 0.0)
    scale_new = jnp.exp(top_two - top_new)
    memory_new = scale_old[:, None, None] * memory_one + scale_new[:, None, None] * memory_two
    normal_new = scale_old[:, None] * normal_one + scale_new[:, None] * normal_two
    decay_new = jnp.where(keep, decay_one + decay_step, decay_two)
    first_new = jnp.where(earlier_empty, first_two, first_one)
    last_new = jnp.where(later_empty, last_one, last_two)
    return (memory_new, normal_new, top_new, decay_new, first_new, last_new)


def block_summary(key_block, value_block, gate_block, decay_block, segment):
    cumulative = jnp.cumsum(decay_block, axis=-1)
    latest = segment == segment[-1]
    growth = jnp.where(latest[None, :], cumulative[:, -1:] - cumulative + gate_block, very_negative)
    top_log = jnp.max(growth, axis=-1)
    weight_table = jnp.exp(growth - top_log[:, None])
    key_expanded = key_block.astype(jnp.float32)
    value_expanded = value_block.astype(jnp.float32)
    memory_matrix = jnp.einsum(
        "jw,wjm,wju->jmu",
        weight_table,
        key_expanded,
        value_expanded,
        precision=lax.Precision.HIGHEST,
    )
    normal = jnp.einsum("hs,shk->hk", weight_table, key_expanded, precision=lax.Precision.HIGHEST)
    return (memory_matrix, normal, top_log, cumulative[:, -1], segment[0], segment[-1])


def block_output(query_block, key_block, value_block, gate_block, decay_block, segment, state):
    memory_matrix, normal, top_log, total_decay, first_doc, last_doc = state
    head_dim = query_block.shape[2]
    length = segment.shape[0]
    cumulative = jnp.cumsum(decay_block, axis=-1)
    row_ids = lax.broadcasted_iota(jnp.int32, (length, length), 0)
    col_ids = lax.broadcasted_iota(jnp.int32, (length, length), 1)
    allowed = (col_ids <= row_ids) & (segment[:, None] == segment[None, :])
    inside = jnp.where(
        allowed[None],
        cumulative[:, :, None] - cumulative[:, None, :] + gate_block[:, None, :],
        very_negative,
    )
    outside = jnp.where(
        (segment == last_doc)[None, :], cumulative + top_log[:, None], very_negative
    )
    peak_log = jnp.maximum(outside, jnp.max(inside, axis=-1))
    carried = jnp.exp(outside - peak_log)
    scaled = query_block * jnp.asarray(head_dim ** (-0.5), query_block.dtype)
    scores = jnp.einsum("lhd,shd->hls", scaled, key_block, preferred_element_type=jnp.float32)
    weight_table = jnp.exp(inside - peak_log[:, :, None]) * scores
    from_block = jnp.einsum(
        "hls,shv->hlv",
        weight_table.astype(jnp.bfloat16),
        value_block,
        preferred_element_type=jnp.float32,
    )
    scaled_expanded = scaled.astype(jnp.float32)
    memory_readout = jnp.einsum(
        "pug,uga->upa", scaled_expanded, memory_matrix, precision=lax.Precision.HIGHEST
    )
    numer_part = carried[:, :, None] * memory_readout + from_block
    denom_part = carried * jnp.einsum(
        "lhk,hk->hl", scaled_expanded, normal, precision=lax.Precision.HIGHEST
    ) + jnp.sum(weight_table, axis=-1)
    result = numer_part / jnp.maximum(jnp.abs(denom_part), jnp.exp(-peak_log))[:, :, None]
    return jnp.transpose(result, (1, 0, 2)).reshape(length, -1).astype(jnp.bfloat16)


def on_device(
    residual,
    query_vectors,
    key_vectors,
    value_vectors,
    in_gate,
    forget_gate,
    documents,
    w_out,
    norm_gain,
    w_up,
    w_down,
):
    tok_rows = query_vectors.shape[0]
    local_heads = in_gate.shape[0]
    head_dim = query_vectors.shape[1] // local_heads
    block_count = tok_rows // SPAN

    def to_blocks(vectors):
        return vectors.reshape(block_count, SPAN, local_heads, head_dim)

    def gate_blocks(gates):
        return jnp.transpose(gates.reshape(local_heads, block_count, SPAN), (1, 0, 2))

    query_blocks = to_blocks(query_vectors)
    key_blocks = to_blocks(key_vectors)
    value_blocks = to_blocks(value_vectors)
    input_blocks = gate_blocks(in_gate)
    decay_blocks = gate_blocks(jax.nn.log_sigmoid(forget_gate))
    segments = documents.astype(jnp.float32).reshape(block_count, SPAN)
    summaries = jax.vmap(block_summary)(
        key_blocks, value_blocks, input_blocks, decay_blocks, segments
    )
    empty_state = identity_state(local_heads, head_dim)

    def prefix_step(state, summary):
        return (combine(state, summary), state)

    device_total, prefixes = lax.scan(prefix_step, empty_state, summaries)
    incoming = carried_in(device_total, "sp", combine, empty_state)
    entering = jax.vmap(combine, in_axes=(None, 0))(incoming, prefixes)
    mixed = jax.vmap(block_output)(
        query_blocks, key_blocks, value_blocks, input_blocks, decay_blocks, segments, entering
    )
    mixed = mixed.reshape(tok_rows, local_heads * head_dim)
    regrouped = lax.all_to_all(mixed, "tp", split_axis=0, concat_axis=1, tiled=True)
    columns = regrouped
    projected = jnp.dot(
        columns, lax.all_gather(w_out, "tp", axis=0, tiled=True), preferred_element_type=jnp.float32
    )
    middle = (residual.astype(jnp.float32) + projected).astype(jnp.bfloat16)
    middle_wide = middle.astype(jnp.float32)
    factor = lax.rsqrt(jnp.mean(middle_wide * middle_wide, axis=-1, keepdims=True) + epsilon)
    normed = (middle_wide * factor * norm_gain.astype(jnp.float32)).astype(jnp.bfloat16)
    gathered = lax.all_gather(normed, "tp", axis=0, tiled=True)
    columns = gathered
    lifted = jnp.dot(
        columns, lax.all_gather(w_up, "sp", axis=0, tiled=True), preferred_element_type=jnp.float32
    )
    hidden = jnp.square(jax.nn.relu(lifted)).astype(jnp.bfloat16)
    terms = jnp.dot(
        hidden, lax.all_gather(w_down, "sp", axis=1, tiled=True), preferred_element_type=jnp.float32
    )
    summed = lax.psum_scatter(
        terms.astype(jnp.bfloat16), "tp", scatter_dimension=0, tiled=True
    ).astype(jnp.float32)
    return (middle_wide + summed).astype(jnp.bfloat16)


def solution(mesh):
    placed = (
        P(("sp", "tp"), None),
        P("sp", "tp"),
        P("sp", "tp"),
        P("sp", "tp"),
        P("tp", "sp"),
        P("tp", "sp"),
        P("sp"),
        P("tp", None),
        P(),
        P("sp", "tp"),
        P("tp", "sp"),
    )
    return jax.shard_map(
        on_device, mesh=mesh, in_specs=placed, out_specs=P(("sp", "tp"), None), check_vma=False
    )
```

profile of v0, /device:TPU:0, one launch (start us, length us, event | category | flops | bytes accessed | tf_op | source)
XLA Modules:
  0.0 511.1 jit_solution(8846787200100752153)
XLA Ops:
  12.2 1.0 copy.53
  13.2 1.1 reshape.152
  15.3 11.2 %while.55 = (s32[]{:T(128)}, f32[4,64,64]{2,1,0:T(8,128)S(1)}, f32[4,64]{1,0:T(4,128)S(1)}, f32[4]{0:T(128)S(1)}, f32[4]{0:T(128)S(1)}, /*index=5*/f32[]{:T(128)...) while((s32[]{:T(128)}, f32[4,64,64]{2,1,0:T(8,128)S(1)}, ...), condition=%wide.region_3.4_spmd.clone.clone, body=%wide.region_2.3_spmd.clone.sunk.clone | while | flops 83255 | bytes 466630 | solution.py:155
  30.9 35.2 %all-reduce.4 = (f32[16]{0:T(128)S(1)}, f32[16]{0:T(128)S(1)}, f32[64]{0:T(128)S(1)}, f32[64]{0:T(128)S(1)}) all-reduce(f32[16]{0:T(128)S(1)} %dynamic-update-slice, f32[16]{0:T(128)S(1)} %dynamic-update-slice.1, f32[64]{0:T(128)S(1)} %dynamic-update-slice.2, f32[64]{0:T(128)S(1)} %dynamic-update-slice.3), channel_id=1, replica_groups=mesh['sp'=16,'tp'=2] {'sp'}, use_global_device_ids=true, to_apply=%add | all-reduce | flops 160 | bytes 1280
  66.3 17.2 %all-gather.4 = f32[16,4,64]{2,1,0:T(4,128)S(1)} all-gather(f32[1,4,64]{2,1,0:T(4,128)S(1)} %bitcast.198), channel_id=5, replica_groups=mesh['sp'=16,'tp'=2] {'sp'}, dimensions={0}, use_global_device_ids=true | all-gather | bytes 17408 | tf_op jit(solution)/shard_map/all_gather | solution.py:15
  84.4 91.4 %while.56 = (s32[]{:T(128)}, f32[4,64,64]{2,1,0:T(8,128)S(1)}, f32[4,64]{1,0:T(4,128)S(1)}, f32[4]{0:T(128)S(1)}, f32[]{:T(128)}, /*index=5*/s32[]{:T(128)}, f32...) while((s32[]{:T(128)}, f32[4,64,64]{2,1,0:T(8,128)S(1)}, ...), condition=%wide.region_5.6_spmd.clone.clone, body=%wide.region_4.5_spmd.clone.sunk.clone | while | flops 83247 | bytes 200163 | solution.py:27
  88.3 1.0 fusion.70
  94.0 1.0 fusion.70
  99.7 1.0 fusion.70
  105.4 1.0 fusion.70
  111.2 1.0 fusion.70
  116.9 1.0 fusion.70
  122.6 1.0 fusion.70
  128.3 1.0 fusion.70
  134.0 1.0 fusion.70
  139.7 1.0 fusion.70
  145.4 1.0 fusion.70
  151.1 1.0 fusion.70
  156.8 1.0 fusion.70
  162.6 1.0 fusion.70
  168.3 1.0 fusion.70
  174.0 1.0 fusion.70
  178.2 3.4 all-to-all-start
  181.7 4.5 all-to-all-done
  186.2 2.1 multiply_reduce_fusion
  188.3 1.0 multiply_convert_fusion
  190.5 18.0 %all-gather.13.cloned.1.call-done = bf16[256,2048]{1,0:T(8,128)(2,1)} async-done(((bf16[128,2048]{1,0:T(8,128)(2,1)}), bf16[256,2048]{1,0:T(8,128)(2,1)}) %all-gather.13.cloned.1.call-update) | async-done | bytes 1048592 | tf_op jit(solution)/shard_map/all_gather | solution.py:171
  208.5 128.5 %all-gather.15.cloned.1.call-done = bf16[2048,4096]{1,0:T(8,128)(2,1)} async-done(((bf16[128,4096]{1,0:T(8,128)(2,1)}), bf16[2048,4096]{1,0:T(8,128)(2,1)}) %all-gather.15.cloned.1.call-update) | async-done | bytes 16777232 | tf_op jit(solution)/shard_map/all_gather | solution.py:174
  337.0 130.1 %all-gather.17.cloned.1.call-done = bf16[4096,2048]{1,0:T(8,128)(2,1)} async-done(((bf16[4096,128]{1,0:T(8,128)(2,1)}), bf16[4096,2048]{1,0:T(8,128)(2,1)}) %all-gather.17.cloned.1.call-update) | async-done | bytes 16777232 | tf_op jit(solution)/shard_map/all_gather | solution.py:178
  467.1 16.5 %convolution_convert_fusion = bf16[256,2048]{1,0:T(8,128)(2,1)} fusion(bf16[4096,2048]{1,0:T(8,128)(2,1)} %all-gather.17.cloned.1.call-done, bf16[256,2048]{1,0:T(8,128)(2,1)} %all-gather.13.cloned.1.call-done, bf16[2048,4096]{1,0:T(8,128)(2,1)} %all-gather.15.cloned.1.call-done), kind=kOutput, calls=%fused_computation.40 | convolution fusion | flops 8593604608 | bytes 35651584 | tf_op jit(solution)/shard_map/dot_general | solution.py:177
  483.6 18.7 %reduce-scatter.2.cloned.1.call-done = bf16[128,2048]{1,0:T(8,128)(2,1)} async-done(((bf16[256,2048]{1,0:T(8,128)(2,1)}), bf16[128,2048]{1,0:T(8,128)(2,1)}) %reduce-scatter.2.cloned.1.call-update) | async-done | bytes 524304 | tf_op jit(solution)/shard_map/reduce_scatter | solution.py:180
  502.3 2.0 add_convert_fusion
  (193 shorter events, 40.1 us)
Async XLA Ops:
  6.5 21.5 %copy-start.6 = (u32[32]{0:T(128)S(1)}, u32[32]{0:T(128)}, u32[]{:S(2)}) copy-start(u32[32]{0:T(128)} %constant.91) | copy-start | bytes 388
  6.5 77.0 %copy-start.2 = (bf16[256,256]{1,0:T(8,128)(2,1)S(1)}, bf16[256,256]{1,0:T(8,128)(2,1)}, u32[]{:S(2)}) copy-start(bf16[256,256]{1,0:T(8,128)(2,1)} %param.16) | copy-start | bytes 393220
  6.5 77.8 %all-gather.19.cloned.1.call-start = ((), (), s32[]{:S(2)}) async-start(), calls=%async_computation.7 | async-start | bytes 2228224 | tf_op jit(solution)/shard_map/all_gather | solution.py:15
  13.2 70.8 %copy-start.3 = (f32[4,256]{1,0:T(4,128)S(1)}, f32[4,256]{1,0:T(4,128)}, u32[]{:S(2)}) copy-start(f32[4,256]{1,0:T(4,128)} %param.19) | copy-start | bytes 12292
  15.2 160.6 %copy-start.4 = (s32[256]{0:T(256)S(1)}, s32[256]{0:T(256)}, u32[]{:S(2)}) copy-start(s32[256]{0:T(256)} %param.21) | copy-start | bytes 3076
  26.5 0.7 copy-start
  27.2 154.5 %copy-start.5 = (bf16[2048]{0:T(1024)(128)(2,1)S(1)}, bf16[2048]{0:T(1024)(128)(2,1)}, u32[]{:S(2)}) copy-start(bf16[2048]{0:T(1024)(128)(2,1)} %param.23) | copy-start | bytes 12292
  27.2 159.0 %copy-start.1 = (bf16[128,2048]{1,0:T(8,128)(2,1)S(1)}, bf16[128,2048]{1,0:T(8,128)(2,1)}, u32[]{:S(2)}) copy-start(bf16[128,2048]{1,0:T(8,128)(2,1)} %param.15) | copy-start | bytes 1572868
  27.2 159.0 %all-gather.11.cloned.1.call-start = ((), (), s32[]{:S(2)}) async-start(), calls=%async_computation.2 | async-start | bytes 3145728 | tf_op jit(solution)/shard_map/all_gather | solution.py:165
  178.2 7.9 %all-to-all-start = ((bf16[2,128,256]{1,2,0:T(8,128)(2,1)}), bf16[2,128,256]{1,2,0:T(8,128)(2,1)S(1)}, u32[]{:S(2)}, u32[]{:S(2)}) async-start(bf16[2,128,256]{1,2,0:T(8,128)(2,1)} %bitcast.27), calls=%async_computation | async-start | bytes 262144 | tf_op jit(solution)/shard_map/all_to_all | solution.py:162
  181.6 26.9 %all-gather.13.cloned.1.call-start = ((), (), s32[]{:S(2)}) async-start(), calls=%async_computation.3 | async-start | bytes 1572864 | tf_op jit(solution)/shard_map/all_gather | solution.py:171
  189.3 147.7 %all-gather.15.cloned.1.call-start = ((), (), s32[]{:S(2)}) async-start(), calls=%async_computation.4 | async-start | bytes 17825792 | tf_op jit(solution)/shard_map/all_gather | solution.py:174
  189.9 277.2 %all-gather.17.cloned.1.call-start = ((), (), s32[]{:S(2)}) async-start(), calls=%async_computation.5 | async-start | bytes 17825792 | tf_op jit(solution)/shard_map/all_gather | solution.py:178
  190.5 311.8 %reduce-scatter.2.cloned.1.call-start = ((), (), s32[]{:S(2)}) async-start(), calls=%async_computation.6 | async-start | bytes 1572864 | tf_op jit(solution)/shard_map/reduce_scatter | solution.py:180
Sparse Core Ops, SparseCore 0:
  27.3 44.1 all-gather.18
  73.0 31.7 all-gather.10
  189.4 19.0 all-gather.12
  210.5 126.4 all-gather.14
  339.0 128.0 all-gather.16
  483.7 18.5 reduce-scatter.1
where the time goes:
time: 513 us; the launch traced here: 511 us
  waiting for transfers between devices  302 us (59%)
  loops' own time  61.4 us (12%)
  blocking collectives  52.5 us (10%)
  local copies, waits for them, and re-layouts  28.9 us (6%)
  other arithmetic  27.6 us (5%)
  matrix products  21.3 us (4%)
  between operations  14.4 us (3%)
    all_gather x1, waiting for transfers between devices, on_device(): lax.all_gather(w_down, 'sp', axis=1, tiled=True)  130 us
    all_gather x1, waiting for transfers between devices, on_device(): lax.all_gather(w_up, 'sp', axis=0, tiled=True)  128 us
    another operation x1, loops' own time, carried_in(): return lax.fori_loop(0, length, lap, start)  53.6 us
    unnamed x1, blocking collectives  35.2 us
    dynamic_slice x32, local copies, waits for them, and re-layouts, lap(): new = combine(before, jax.tree.map(lambda part: part[k], everything))  19.7 us
    reduce_scatter x1, waiting for transfers between devices, on_device(): lax.psum_scatter(terms.astype(jnp.bfloat16), 'tp', scatter_dimension=0, t...  18.7 us
    all_gather x1, waiting for transfers between devices, on_device(): gathered = lax.all_gather(normed, 'tp', axis=0, tiled=True)  18 us
    select_n x48, other arithmetic, lap(): return jax.tree.map(lambda a, b: jnp.where(reached, a, b), new, before)  17.7 us
  transfers between devices with their start and end apart: 7, of which 5 were waited for; matrix products, arithmetic and copies ran while one was open for 9% of the time, Pallas kernels for 0%

commit v1 on v0

v1 whole, which is shorter than its diff:
```python
import jax
import jax.numpy as jnp
import numpy as np
from jax import lax
from jax.sharding import Mesh, PartitionSpec as P

DOC_MOST = 2048
very_negative = -1e30
epsilon = 1e-06
SP = ("z", "g")


def combine(earlier, later):
    memory_one, top_one, decay_one, first_one, last_one = earlier
    memory_two, top_two, decay_two, first_two, last_two = later
    later_empty = first_two < 0.0
    earlier_empty = first_one < 0.0
    keep = later_empty | (first_two == last_two) & (first_two == last_one)
    decay_step = jnp.where(later_empty, 0.0, decay_two)
    top_new = jnp.where(keep, jnp.maximum(decay_step + top_one, top_two), top_two)
    scale_old = jnp.where(keep, jnp.exp(decay_step + top_one - top_new), 0.0)
    scale_new = jnp.exp(top_two - top_new)
    memory_new = scale_old[:, None, None] * memory_one + scale_new[:, None, None] * memory_two
    decay_new = jnp.where(keep, decay_one + decay_step, decay_two)
    first_new = jnp.where(earlier_empty, first_two, first_one)
    last_new = jnp.where(later_empty, last_one, last_two)
    return (memory_new, top_new, decay_new, first_new, last_new)


def pack(state):
    memory, top, decay, first, last = state
    heads, _, width = memory.shape
    row = jnp.stack(
        [top, decay, jnp.broadcast_to(first, top.shape), jnp.broadcast_to(last, top.shape)], axis=1
    )
    row = jnp.pad(row, ((0, 0), (0, width - 4)))
    return jnp.concatenate(
        [memory, row[:, None, :], jnp.zeros((heads, 6, width), jnp.float32)], axis=1
    )


def unpack(packed, present):
    rows = packed.shape[1] - 7
    row = packed[:, rows]
    memory = jnp.where(present, packed[:, :rows], 0.0)
    top = jnp.where(present, row[:, 0], very_negative)
    decay = jnp.where(present, row[:, 1], 0.0)
    first = jnp.where(present, row[0, 2], -1.0)
    last = jnp.where(present, row[0, 3], -1.0)
    return (memory, top, decay, first, last)


def shifted(state, distance, length, here):
    packed = lax.ppermute(pack(state), SP, [(i, i + distance) for i in range(length - distance)])
    return unpack(packed, here >= distance)


def on_device(
    residual,
    query_vectors,
    key_vectors,
    value_vectors,
    in_gate,
    forget_gate,
    documents,
    w_out,
    norm_gain,
    w_up,
    w_down,
):
    tok_rows = query_vectors.shape[0]
    heads = in_gate.shape[0]
    head_dim = query_vectors.shape[1] // heads
    length = lax.axis_size(SP)
    here = lax.axis_index(SP)
    tp = lax.axis_size("tp")
    me = lax.axis_index("tp")

    up_part = lax.all_to_all(w_up, "g", split_axis=1, concat_axis=0, tiled=True)
    down_part = lax.all_to_all(w_down, "g", split_axis=0, concat_axis=1, tiled=True)
    up_all = lax.all_gather(up_part, "z", axis=0, tiled=True)

    def turn(value, d):
        return lax.ppermute(value, "tp", [(i, (i + d) % tp) for i in range(tp)])

    w_out_parts = [w_out] + [turn(w_out, d) for d in range(1, tp)]

    segment = documents.astype(jnp.float32)
    decay_log = jax.nn.log_sigmoid(forget_gate)
    cumulative = jnp.cumsum(decay_log, axis=-1)
    key_heads = jnp.transpose(key_vectors.reshape(tok_rows, heads, head_dim), (1, 0, 2))
    value_heads = jnp.transpose(value_vectors.reshape(tok_rows, heads, head_dim), (1, 0, 2))
    query_heads = jnp.transpose(query_vectors.reshape(tok_rows, heads, head_dim), (1, 0, 2))
    query_heads = query_heads * jnp.asarray(head_dim ** (-0.5), query_heads.dtype)
    latest = segment == segment[-1]
    growth = jnp.where(latest[None, :], cumulative[:, -1:] - cumulative + in_gate, very_negative)
    top_log = jnp.max(growth, axis=-1)
    summary_weight = jnp.exp(growth - top_log[:, None])
    key_wide = key_heads.astype(jnp.float32)
    weighted = key_wide * summary_weight[:, :, None]
    memory = jnp.einsum(
        "hsv,hsk->hvk", value_heads.astype(jnp.float32), weighted, precision=lax.Precision.HIGHEST
    )
    normal = jnp.sum(weighted, axis=1)
    state = (
        jnp.concatenate([memory, normal[:, None, :]], axis=1),
        top_log,
        cumulative[:, -1],
        segment[0],
        segment[-1],
    )

    reach = min(length - 1, -(-(DOC_MOST - 1) // tok_rows))
    span = 1
    while span < reach:
        state = combine(shifted(state, span, length, here), state)
        span *= 2
    incoming = shifted(state, 1, length, here)
    memory_in, top_in, _, _, last_in = incoming

    row_ids = lax.broadcasted_iota(jnp.int32, (tok_rows, tok_rows), 0)
    col_ids = lax.broadcasted_iota(jnp.int32, (tok_rows, tok_rows), 1)
    allowed = (col_ids <= row_ids) & (segment[:, None] == segment[None, :])
    inside = jnp.where(
        allowed[None],
        cumulative[:, :, None] - cumulative[:, None, :] + in_gate[:, None, :],
        very_negative,
    )
    peak_inside = jnp.max(inside, axis=-1)
    scores = jnp.einsum(
        "hld,hsd->hls", query_heads, key_heads, preferred_element_type=jnp.float32
    )
    weight_inside = jnp.exp(inside - peak_inside[:, :, None]) * scores
    from_block = jnp.einsum(
        "hls,hsv->hlv",
        weight_inside.astype(jnp.bfloat16),
        value_heads,
        preferred_element_type=jnp.float32,
    )
    sum_inside = jnp.sum(weight_inside, axis=-1)

    outside = jnp.where((segment == last_in)[None, :], cumulative + top_in[:, None], very_negative)
    peak_log = jnp.maximum(outside, peak_inside)
    carried = jnp.exp(outside - peak_log)
    local = jnp.exp(peak_inside - peak_log)
    readout = jnp.einsum(
        "hlk,hvk->hlv",
        query_heads.astype(jnp.float32),
        memory_in,
        precision=lax.Precision.HIGHEST,
    )
    numer = carried[:, :, None] * readout[:, :, :head_dim] + local[:, :, None] * from_block
    denom = carried * readout[:, :, head_dim] + local * sum_inside
    mixed = numer / jnp.maximum(jnp.abs(denom), jnp.exp(-peak_log))[:, :, None]
    mixed = jnp.transpose(mixed, (1, 0, 2)).reshape(tok_rows, -1).astype(jnp.bfloat16)

    own_rows = tok_rows // tp
    mixed_rows = mixed.reshape(tp, own_rows, -1)
    projected = 0.0
    for d in range(tp):
        piece = lax.dynamic_index_in_dim(mixed_rows, (me + d) % tp, 0, keepdims=False)
        if d:
            piece = turn(piece, d)
        projected = projected + jnp.dot(
            piece, w_out_parts[d], preferred_element_type=jnp.float32
        )
    middle = (residual.astype(jnp.float32) + projected).astype(jnp.bfloat16)
    middle_wide = middle.astype(jnp.float32)
    factor = lax.rsqrt(jnp.mean(middle_wide * middle_wide, axis=-1, keepdims=True) + epsilon)
    normed = (middle_wide * factor * norm_gain.astype(jnp.float32)).astype(jnp.bfloat16)

    gathered = lax.all_gather(normed, ("g", "tp"), axis=0, tiled=True)
    down_all = lax.all_gather(down_part, "z", axis=1, tiled=True)
    lifted = jnp.dot(gathered, up_all, preferred_element_type=jnp.float32)
    hidden = jnp.square(jax.nn.relu(lifted)).astype(jnp.bfloat16)
    terms = jnp.dot(hidden, down_all, preferred_element_type=jnp.float32)
    summed = lax.psum_scatter(
        terms.astype(jnp.bfloat16), ("g", "tp"), scatter_dimension=0, tiled=True
    ).astype(jnp.float32)
    return (middle_wide + summed).astype(jnp.bfloat16)


def solution(mesh):
    sp, tp = mesh.shape["sp"], mesh.shape["tp"]
    plane = min(sp, 2 * tp)
    if sp % plane:
        plane = 1
    split = Mesh(np.asarray(mesh.devices).reshape(sp // plane, plane, tp), ("z", "g", "tp"))
    placed = (
        P(("z", "g", "tp"), None),
        P(SP, "tp"),
        P(SP, "tp"),
        P(SP, "tp"),
        P("tp", SP),
        P("tp", SP),
        P(SP),
        P("tp", None),
        P(),
        P(SP, "tp"),
        P("tp", SP),
    )
    return jax.shard_map(
        on_device,
        mesh=split,
        in_specs=placed,
        out_specs=P(("z", "g", "tp"), None),
        check_vma=False,
    )
```

time: 513 us -> 309 us (0.60)
  waiting for transfers between devices: 302 us -> 206 us
  loops' own time: 61.4 us -> 0 us
  blocking collectives: 52.5 us -> 18.8 us
  other arithmetic: 27.6 us -> 8.61 us
  starting transfers between devices: 3.58 us -> 22.2 us
  local copies, waits for them, and re-layouts: 28.9 us -> 13.7 us
  between operations: 14.4 us -> 21.6 us
    all_gather x5 -> x3, waiting for transfers between devices: 277 us -> 142 us  [the longest x1 88.8 us: on_device(): up_all = lax.all_gather(up_part, 'z', axis=0, tiled=True)]
    another operation x2 -> x0, loops' own time: 61.4 us -> none  [the longest x1 53.6 us: carried_in(): return lax.fori_loop(0, length, lap, start)]
    unnamed x1 -> x0, blocking collectives: 35.2 us -> none
    reduce_scatter x1, waiting for transfers between devices: 18.7 us -> 51.3 us  [on_device(): lax.psum_scatter(terms.astype(jnp.bfloat16), ('g', 'tp'), scatter_dimensi...]
    dynamic_slice x36 -> x1, local copies, waits for them, and re-layouts: 22.2 us -> 0.28 us  [on_device(): lax.dynamic_index_in_dim(mixed_rows, (me + d) % tp, 0, keepdims=False)]
    all_to_all x0 -> x1, blocking collectives: none -> 18.8 us  [on_device(): lax.all_to_all(w_down, 'g', split_axis=0, concat_axis=1, tiled=True)]
    ppermute x0 -> x6, starting transfers between devices: none -> 17.4 us  [the longest x4 15.2 us: shifted(): lax.ppermute(pack(state), SP, [(i, i + distance) for i in range(length -...]
    all_gather x1 -> x0, blocking collectives: 17.2 us -> none  [carried_in(): everything = jax.tree.map(lambda part: lax.all_gather(part, axis), value)]
  transfers between devices with their start and end apart: 7 -> 11, of which waited for: 5 -> 8; matrix products, arithmetic and copies ran while one was open for 9% -> 7% of each run, Pallas kernels for 0% -> 0%
where the time goes in v1:
time: 309 us
  waiting for transfers between devices  206 us (67%)
  starting transfers between devices  22.2 us (7%)
  between operations  21.6 us (7%)
  blocking collectives  18.8 us (6%)
  matrix products  17.7 us (6%)
  local copies, waits for them, and re-layouts  13.7 us (4%)
  other arithmetic  8.61 us (3%)
    all_gather x1, waiting for transfers between devices, on_device(): up_all = lax.all_gather(up_part, 'z', axis=0, tiled=True)  88.8 us
    reduce_scatter x1, waiting for transfers between devices, on_device(): lax.psum_scatter(terms.astype(jnp.bfloat16), ('g', 'tp'), scatter_dimensi...  51.3 us
    all_gather x1, waiting for transfers between devices, on_device(): gathered = lax.all_gather(normed, ('g', 'tp'), axis=0, tiled=True)  37 us
    all_to_all x1, blocking collectives, on_device(): lax.all_to_all(w_down, 'g', split_axis=0, concat_axis=1, tiled=True)  18.8 us
    all_gather x1, waiting for transfers between devices, on_device(): down_all = lax.all_gather(down_part, 'z', axis=1, tiled=True)  16.1 us
    ppermute x4, starting transfers between devices, shifted(): lax.ppermute(pack(state), SP, [(i, i + distance) for i in range(length -...  15.2 us
    dot_general x1, matrix products, on_device(): terms = jnp.dot(hidden, down_all, preferred_element_type=jnp.float32)  14.4 us
    ppermute x4, waiting for transfers between devices, shifted(): lax.ppermute(pack(state), SP, [(i, i + distance) for i in range(length -...  9.54 us
  transfers between devices with their start and end apart: 11, of which 8 were waited for; matrix products, arithmetic and copies ran while one was open for 7% of the time, Pallas kernels for 0%

profile of v1, /device:TPU:0, one launch (start us, length us, event | category | flops | bytes accessed | tf_op | source)
XLA Modules:
  0.0 308.7 jit_solution(7243872329865839913)
XLA Ops:
  6.6 18.8 %all_to_all.38 = bf16[4,1024,128]{2,1,0:T(8,128)(2,1)S(1)} all-to-all(bf16[4,1024,128]{2,1,0:T(8,128)(2,1)} %bitcast.89), channel_id=1, replica_groups=mesh['z'=4,'g'=4,'tp'=2] {'g'}, dimensions={0} | all-to-all | bytes 2097152 | tf_op jit(solution)/shard_map/all_to_all | solution.py:80
  25.4 1.4 copy.209
  27.5 0.6 pad.46.clone
  28.1 0.7 pad.47.clone
  28.9 1.2 reduce-window.6
  32.2 1.0 copy.193
  33.7 2.0 collective-permute-start
  35.7 1.3 copy.207
  37.0 4.7 %all-to-all-start = ((bf16[128,4,1024]{0,2,1:T(8,128)(2,1)}), bf16[128,4,1024]{0,2,1:T(8,128)(2,1)S(1)}, u32[]{:S(2)}, u32[]{:S(2)}) async-start(bf16[128,4,1024]{0,2,1:T(8,128)(2,1)} %bitcast.30), calls=%async_computation | async-start | bytes 2097152 | tf_op jit(solution)/shard_map/all_to_all | solution.py:79
  41.7 1.6 collective-permute-start.5
  45.3 1.1 slice_reduce_fusion.3
  46.3 0.7 fusion.46
  50.7 1.0 fusion.16
  51.8 3.9 %collective-permute-start.1 = (f32[4,72,64]{1,2,0:T(8,128)S(1)}, f32[4,72,64]{1,2,0:T(8,128)S(1)}, u32[]{:S(2)}, u32[]{:S(2)}) collective-permute-start(f32[4,72,64]{1,2,0:T(8,128)S(1)} %maximum_maximum_fusion.1), channel_id=1, source_target_pairs={{0,4},{2,6},{4,8},{6,10},{8,12},{10,14},{12,16},{14,18},{16,20},{1... | collective-permute-start | bytes 221192 | tf_op jit(solution)/shard_map/ppermute | solution.py:54
  56.1 3.0 collective-permute-done.1
  59.2 0.7 fusion.45
  60.5 1.3 copy.208
  63.3 8.0 %collective-permute-start.2 = (f32[4,72,64]{1,2,0:T(8,128)S(1)}, f32[4,72,64]{1,2,0:T(8,128)S(1)}, u32[]{:S(2)}, u32[]{:S(2)}) collective-permute-start(f32[4,72,64]{1,2,0:T(8,128)S(1)} %maximum_maximum_fusion.2), channel_id=1, source_target_pairs={{0,8},{2,10},{4,12},{6,14},{8,16},{10,18},{12,20},{14,22},{16,24},... | collective-permute-start | bytes 221192 | tf_op jit(solution)/shard_map/ppermute | solution.py:54
  71.9 5.7 %collective-permute-done.2 = f32[4,72,64]{1,2,0:T(8,128)S(1)} collective-permute-done((f32[4,72,64]{1,2,0:T(8,128)S(1)}, f32[4,72,64]{1,2,0:T(8,128)S(1)}, u32[]{:S(2)}, u32[]{:S(2)}) %collective-permute-start.2) | collective-permute-done | bytes 73760 | tf_op jit(solution)/shard_map/ppermute | solution.py:54
  77.7 0.7 fusion.44
  80.5 1.3 collective-permute-start.3
  81.9 0.9 collective-permute-done.3
  82.9 0.6 slice.113
  86.6 3.4 %collective-permute-done.4 = bf16[128,256]{1,0:T(8,128)(2,1)S(1)} collective-permute-done((bf16[128,256]{1,0:T(8,128)(2,1)S(1)}, bf16[128,256]{1,0:T(8,128)(2,1)S(1)}, u32[]{:S(2)}, u32[]{:S(2)}) %collective-permute-start.4) | collective-permute-done | bytes 65568 | tf_op jit(solution)/shard_map/ppermute | solution.py:84
  90.0 1.6 multiply_reduce_fusion
  91.6 1.0 multiply_convert_fusion.1
  92.7 16.1 %all-gather.8.cloned.1.call-done = bf16[1024,2048]{0,1:T(8,128)(2,1)} async-done(((bf16[1024,512]{0,1:T(8,128)(2,1)}), bf16[1024,2048]{0,1:T(8,128)(2,1)}) %all-gather.8.cloned.1.call-update) | async-done | bytes 4194320 | tf_op jit(solution)/shard_map/all_gather | solution.py:173
  108.7 88.8 %all-gather.6.cloned.1.call-done = bf16[2048,1024]{1,0:T(8,128)(2,1)} async-done(((bf16[512,1024]{1,0:T(8,128)(2,1)}), bf16[2048,1024]{1,0:T(8,128)(2,1)}) %all-gather.6.cloned.1.call-update) | async-done | bytes 4194320 | tf_op jit(solution)/shard_map/all_gather | solution.py:81
  197.6 37.0 %all-gather.4.cloned.1.call-done = bf16[1024,2048]{1,0:T(8,128)(2,1)} async-done(((bf16[128,2048]{1,0:T(8,128)(2,1)}), bf16[1024,2048]{1,0:T(8,128)(2,1)}) %all-gather.4.cloned.1.call-update) | async-done | bytes 4194320 | tf_op jit(solution)/shard_map/all_gather | solution.py:172
  234.6 14.4 %convolution_convert_fusion = bf16[1024,2048]{1,0:T(8,128)(2,1)} fusion(bf16[1024,2048]{0,1:T(8,128)(2,1)} %all-gather.8.cloned.1.call-done, bf16[1024,2048]{1,0:T(8,128)(2,1)} %all-gather.4.cloned.1.call-done, bf16[2048,1024]{1,0:T(8,128)(2,1)} %all-gather.6.cloned.1.call-done), kind=kOutput, calls=%fused_computation.1 | convolution fusion | flops 8595177472 | bytes 16777216 | tf_op jit(solution)/shard_map/dot_general | solution.py:176
  249.0 51.3 %reduce-scatter.2.cloned.1.call-done = bf16[128,2048]{1,0:T(8,128)(2,1)} async-done(((bf16[1024,2048]{1,0:T(8,128)(2,1)}), bf16[128,2048]{1,0:T(8,128)(2,1)}) %reduce-scatter.2.cloned.1.call-update) | async-done | bytes 524304 | tf_op jit(solution)/shard_map/reduce_scatter | solution.py:177
  300.3 1.9 add_convert_fusion
  (112 shorter events, 9.6 us)
Async XLA Ops:
  6.5 20.3 %copy-start.8 = (s32[256]{0:T(256)S(1)}, s32[256]{0:T(256)}, u32[]{:S(2)}) copy-start(s32[256]{0:T(256)} %param.17) | copy-start | bytes 3076
  6.5 22.3 %copy-start.10 = (f32[4,256]{1,0:T(4,128)S(1)}, f32[4,256]{1,0:T(4,128)}, u32[]{:S(2)}) copy-start(f32[4,256]{1,0:T(4,128)} %param.16) | copy-start | bytes 12292
  6.5 24.8 %copy-start.7 = (f32[4,256]{1,0:T(4,128)S(1)}, f32[4,256]{1,0:T(4,128)}, u32[]{:S(2)}) copy-start(f32[4,256]{1,0:T(4,128)} %param.15) | copy-start | bytes 12292
  6.5 25.2 %copy-start.5 = (bf16[256,256]{1,0:T(8,128)(2,1)S(1)}, bf16[256,256]{1,0:T(8,128)(2,1)}, u32[]{:S(2)}) copy-start(bf16[256,256]{1,0:T(8,128)(2,1)} %param.13) | copy-start | bytes 393220
  6.5 29.2 %copy-start = (bf16[128,4096]{1,0:T(8,128)(2,1)S(1)}, bf16[128,4096]{1,0:T(8,128)(2,1)}, u32[]{:S(2)}) copy-start(bf16[128,4096]{1,0:T(8,128)(2,1)} %param.20) | copy-start | bytes 3145732
  6.5 102.2 %all-gather.8.cloned.1.call-start = ((), (), s32[]{:S(2)}) async-start(), calls=%async_computation.5 | async-start | bytes 5242880 | tf_op jit(solution)/shard_map/all_gather | solution.py:173
  25.4 16.3 %copy-start.1 = (bf16[256,2048]{1,0:T(8,128)(2,1)S(1)}, bf16[256,2048]{1,0:T(8,128)(2,1)}, u32[]{:S(2)}) copy-start(bf16[256,2048]{1,0:T(8,128)(2,1)} %param.18) | copy-start | bytes 3145732
  26.8 16.5 %copy-start.6 = (bf16[256,256]{1,0:T(8,128)(2,1)S(1)}, bf16[256,256]{1,0:T(8,128)(2,1)}, u32[]{:S(2)}) copy-start(bf16[256,256]{1,0:T(8,128)(2,1)} %param.12) | copy-start | bytes 393220
  33.2 3.7 %copy-start.2 = (bf16[256,256]{0,1:T(8,128)(2,1)}, bf16[256,256]{0,1:T(8,128)(2,1)S(1)}, u32[]{:S(2)}) copy-start(bf16[256,256]{0,1:T(8,128)(2,1)S(1)} %copy.193) | copy-start | bytes 393220
  33.7 11.6 %collective-permute-start = (f32[4,72,64]{1,2,0:T(8,128)S(1)}, f32[4,72,64]{1,2,0:T(8,128)}, u32[]{:S(2)}, u32[]{:S(2)}) collective-permute-start(f32[4,72,64]{1,2,0:T(8,128)S(1)} %maximum_maximum_fusion), channel_id=1, source_target_pairs={{0,2},{2,4},{4,6},{6,8},{8,10},{10,12},{12,14},{14,16},{16,18},{18... | collective-permute-start | bytes 221192 | tf_op jit(solution)/shard_map/ppermute | solution.py:54
  37.0 23.5 %all-to-all-start = ((bf16[128,4,1024]{0,2,1:T(8,128)(2,1)}), bf16[128,4,1024]{0,2,1:T(8,128)(2,1)S(1)}, u32[]{:S(2)}, u32[]{:S(2)}) async-start(bf16[128,4,1024]{0,2,1:T(8,128)(2,1)} %bitcast.30), calls=%async_computation | async-start | bytes 2097152 | tf_op jit(solution)/shard_map/all_to_all | solution.py:79
  41.7 155.9 %all-gather.6.cloned.1.call-start = ((), (), s32[]{:S(2)}) async-start(), calls=%async_computation.4 | async-start | bytes 5242880 | tf_op jit(solution)/shard_map/all_gather | solution.py:81
  41.7 48.3 %collective-permute-start.5 = (bf16[256,2048]{1,0:T(8,128)(2,1)S(1)}, bf16[256,2048]{1,0:T(8,128)(2,1)}, u32[]{:S(2)}, u32[]{:S(2)}) collective-permute-start(bf16[256,2048]{1,0:T(8,128)(2,1)S(1)} %copy-done.1), channel_id=1, source_target_pairs={{0,1},{1,0},{2,3},{3,2},{4,5},{5,4},{6,7},{7,6},{8,9},{9,8},{10,11... | collective-permute-start | bytes 3145736 | tf_op jit(solution)/shard_map/ppermute | solution.py:84
  51.7 30.2 %copy-start.9 = (bf16[2048]{0:T(1024)(128)(2,1)S(1)}, bf16[2048]{0:T(1024)(128)(2,1)}, u32[]{:S(2)}) copy-start(bf16[2048]{0:T(1024)(128)(2,1)} %param.19) | copy-start | bytes 12292
  51.8 7.2 %collective-permute-start.1 = (f32[4,72,64]{1,2,0:T(8,128)S(1)}, f32[4,72,64]{1,2,0:T(8,128)S(1)}, u32[]{:S(2)}, u32[]{:S(2)}) collective-permute-start(f32[4,72,64]{1,2,0:T(8,128)S(1)} %maximum_maximum_fusion.1), channel_id=1, source_target_pairs={{0,4},{2,6},{4,8},{6,10},{8,12},{10,14},{12,16},{14,18},{16,20},{1... | collective-permute-start | bytes 221192 | tf_op jit(solution)/shard_map/ppermute | solution.py:54
  60.5 24.4 %copy-start.3 = (bf16[256,256]{0,1:T(8,128)(2,1)S(1)}, bf16[256,256]{0,1:T(8,128)(2,1)}, u32[]{:S(2)}) copy-start(bf16[256,256]{0,1:T(8,128)(2,1)} %copy-done.2) | copy-start | bytes 393220
  61.8 172.7 %all-gather.4.cloned.1.call-start = ((), (), s32[]{:S(2)}) async-start(), calls=%async_computation.3 | async-start | bytes 4718592 | tf_op jit(solution)/shard_map/all_gather | solution.py:172
  63.3 14.2 %collective-permute-start.2 = (f32[4,72,64]{1,2,0:T(8,128)S(1)}, f32[4,72,64]{1,2,0:T(8,128)S(1)}, u32[]{:S(2)}, u32[]{:S(2)}) collective-permute-start(f32[4,72,64]{1,2,0:T(8,128)S(1)} %maximum_maximum_fusion.2), channel_id=1, source_target_pairs={{0,8},{2,10},{4,12},{6,14},{8,16},{10,18},{12,20},{14,22},{16,24},... | collective-permute-start | bytes 221192 | tf_op jit(solution)/shard_map/ppermute | solution.py:54
  71.3 18.7 %copy-start.4 = (bf16[128,2048]{1,0:T(8,128)(2,1)S(1)}, bf16[128,2048]{1,0:T(8,128)(2,1)}, u32[]{:S(2)}) copy-start(bf16[128,2048]{1,0:T(8,128)(2,1)} %param.11) | copy-start | bytes 1572868
  80.5 2.3 collective-permute-start.3
  85.6 4.3 %collective-permute-start.4 = (bf16[128,256]{1,0:T(8,128)(2,1)S(1)}, bf16[128,256]{1,0:T(8,128)(2,1)S(1)}, u32[]{:S(2)}, u32[]{:S(2)}) collective-permute-start(bf16[128,256]{1,0:T(8,128)(2,1)S(1)} %bitcast.94), channel_id=1, source_target_pairs={{0,1},{1,0},{2,3},{3,2},{4,5},{5,4},{6,7},{7,6},{8,9},{9,8},{10,11... | collective-permute-start | bytes 196616 | tf_op jit(solution)/shard_map/ppermute | solution.py:84
  92.6 207.6 %reduce-scatter.2.cloned.1.call-start = ((), (), s32[]{:S(2)}) async-start(), calls=%async_computation.6 | async-start | bytes 4718592 | tf_op jit(solution)/shard_map/reduce_scatter | solution.py:177
Sparse Core Ops, SparseCore 0:
  26.9 81.7 all-gather.7
  110.3 87.2 all-gather.5
  199.5 35.0 all-gather.3
  249.1 51.1 reduce-scatter.1

commit v2 on v1

--- a/solution.py
+++ b/solution.py
@@ -7,7 +7,8 @@
 DOC_MOST = 2048
 very_negative = -1e30
 epsilon = 1e-06
-SP = ("z", "g")
+SP = ("z", "x", "c")
+G = ("x", "c")
 
 
 def combine(earlier, later):
@@ -53,6 +54,21 @@
 def shifted(state, distance, length, here):
     packed = lax.ppermute(pack(state), SP, [(i, i + distance) for i in range(length - distance)])
     return unpack(packed, here >= distance)
+
+
+def turn(value, axis, d):
+    n = lax.axis_size(axis)
+    return lax.ppermute(value, axis, [(i, (i + d) % n) for i in range(n)])
+
+
+def reduced(terms, dim, axis):
+    def block(d):
+        return lax.index_in_dim(terms, d, dim, keepdims=False)
+
+    total = block(0).astype(jnp.float32)
+    for d in range(1, lax.axis_size(axis)):
+        total = total + turn(block(d), axis, -d).astype(jnp.float32)
+    return total.astype(jnp.bfloat16)
 
 
 def on_device(
@@ -76,14 +92,20 @@
     tp = lax.axis_size("tp")
     me = lax.axis_index("tp")
 
-    up_part = lax.all_to_all(w_up, "g", split_axis=1, concat_axis=0, tiled=True)
-    down_part = lax.all_to_all(w_down, "g", split_axis=0, concat_axis=1, tiled=True)
+    plane = lax.axis_size(G)
+    up_pieces = jnp.transpose(w_up.reshape(w_up.shape[0], plane, -1), (1, 0, 2))
+    up_part = lax.all_to_all(up_pieces, G, split_axis=0, concat_axis=0, tiled=True)
+    up_part = up_part.reshape(-1, up_part.shape[-1])
+    up_part, w_down, w_out, key_vectors, in_gate, forget_gate, documents = (
+        lax.optimization_barrier(
+            (up_part, w_down, w_out, key_vectors, in_gate, forget_gate, documents)
+        )
+    )
+    down_part = lax.all_to_all(w_down, G, split_axis=0, concat_axis=1, tiled=True)
     up_all = lax.all_gather(up_part, "z", axis=0, tiled=True)
-
-    def turn(value, d):
-        return lax.ppermute(value, "tp", [(i, (i + d) % tp) for i in range(tp)])
-
-    w_out_parts = [w_out] + [turn(w_out, d) for d in range(1, tp)]
+    down_all = lax.all_gather(down_part, "z", axis=1, tiled=True)
+
+    w_out_parts = [w_out] + [turn(w_out, "tp", d) for d in range(1, tp)]
 
     segment = documents.astype(jnp.float32)
     decay_log = jax.nn.log_sigmoid(forget_gate)
@@ -160,7 +182,7 @@
     for d in range(tp):
         piece = lax.dynamic_index_in_dim(mixed_rows, (me + d) % tp, 0, keepdims=False)
         if d:
-            piece = turn(piece, d)
+            piece = turn(piece, "tp", d)
         projected = projected + jnp.dot(
             piece, w_out_parts[d], preferred_element_type=jnp.float32
         )
@@ -169,25 +191,37 @@
     factor = lax.rsqrt(jnp.mean(middle_wide * middle_wide, axis=-1, keepdims=True) + epsilon)
     normed = (middle_wide * factor * norm_gain.astype(jnp.float32)).astype(jnp.bfloat16)
 
-    gathered = lax.all_gather(normed, ("g", "tp"), axis=0, tiled=True)
-    down_all = lax.all_gather(down_part, "z", axis=1, tiled=True)
+    gathered = normed
+    for axis in ("tp", "x", "c"):
+        gathered = jnp.concatenate(
+            [gathered] + [turn(gathered, axis, d) for d in range(1, lax.axis_size(axis))], axis=0
+        )
     lifted = jnp.dot(gathered, up_all, preferred_element_type=jnp.float32)
     hidden = jnp.square(jax.nn.relu(lifted)).astype(jnp.bfloat16)
-    terms = jnp.dot(hidden, down_all, preferred_element_type=jnp.float32)
-    summed = lax.psum_scatter(
-        terms.astype(jnp.bfloat16), ("g", "tp"), scatter_dimension=0, tiled=True
-    ).astype(jnp.float32)
-    return (middle_wide + summed).astype(jnp.bfloat16)
+    sizes = (lax.axis_size("c"), lax.axis_size("x"), tp)
+    half = down_all.shape[1] // 2
+    summed = []
+    for k, order in enumerate((("c", "x", "tp"), ("c", "tp", "x"))):
+        terms = jnp.dot(
+            hidden, down_all[:, k * half : (k + 1) * half], preferred_element_type=jnp.float32
+        )
+        terms = terms.astype(jnp.bfloat16).reshape(*sizes, own_rows, half)
+        names = ["c", "x", "tp"]
+        for axis in order:
+            terms = reduced(terms, names.index(axis), axis)
+            names.remove(axis)
+        summed.append(terms.astype(jnp.float32))
+    return (middle_wide + jnp.concatenate(summed, axis=1)).astype(jnp.bfloat16)
 
 
 def solution(mesh):
     sp, tp = mesh.shape["sp"], mesh.shape["tp"]
-    plane = min(sp, 2 * tp)
-    if sp % plane:
-        plane = 1
-    split = Mesh(np.asarray(mesh.devices).reshape(sp // plane, plane, tp), ("z", "g", "tp"))
+    chips = tp if sp % (2 * tp) == 0 else 1
+    cores = 2 if sp % 2 == 0 else 1
+    shape = (sp // (chips * cores), chips, cores, tp)
+    split = Mesh(np.asarray(mesh.devices).reshape(shape), ("z", "x", "c", "tp"))
     placed = (
-        P(("z", "g", "tp"), None),
+        P(("z", "x", "c", "tp"), None),
         P(SP, "tp"),
         P(SP, "tp"),
         P(SP, "tp"),
@@ -203,6 +237,6 @@
         on_device,
         mesh=split,
         in_specs=placed,
-        out_specs=P(("z", "g", "tp"), None),
+        out_specs=P(("z", "x", "c", "tp"), None),
         check_vma=False,
     )

time: 309 us -> 251 us (0.81)
  waiting for transfers between devices: 206 us -> 140 us
  starting transfers between devices: 22.2 us -> 45.8 us
  blocking collectives: 18.8 us -> 0 us
    all_gather x1, waiting for transfers between devices: 88.8 us -> 0.01 us  [on_device(): up_all = lax.all_gather(up_part, 'z', axis=0, tiled=True)]
    reduce_scatter x1 -> x0, waiting for transfers between devices: 51.3 us -> none  [on_device(): lax.psum_scatter(terms.astype(jnp.bfloat16), ('g', 'tp'), scatter_dimensi...]
    ppermute x2 -> x11, waiting for transfers between devices: 3.41 us -> 54.5 us  [turn(): return lax.ppermute(value, axis, [(i, (i + d) % n) for i in range(n)])]
    all_gather x1, waiting for transfers between devices: 16.1 us -> 63 us  [on_device(): down_all = lax.all_gather(down_part, 'z', axis=1, tiled=True)]
    all_gather x1 -> x0, waiting for transfers between devices: 37 us -> none  [on_device(): gathered = lax.all_gather(normed, ('g', 'tp'), axis=0, tiled=True)]
    all_to_all x1 -> x0, blocking collectives: 18.8 us -> none  [on_device(): lax.all_to_all(w_down, 'g', split_axis=0, concat_axis=1, tiled=True)]
    all_to_all x1 -> x2, waiting for transfers between devices: 0.01 us -> 18.5 us  [the longest x1 14.1 us: on_device(): lax.all_to_all(up_pieces, G, split_axis=0, concat_axis=0, tiled=True)]
    ppermute x2 -> x11, starting transfers between devices: 2.19 us -> 19.1 us  [turn(): return lax.ppermute(value, axis, [(i, (i + d) % n) for i in range(n)])]
  transfers between devices with their start and end apart: 11 -> 19, of which waited for: 8 -> 13; matrix products, arithmetic and copies ran while one was open for 7% -> 10% of each run, Pallas kernels for 0% -> 0%
where the time goes in v2:
time: 251 us
  waiting for transfers between devices  140 us (56%)
  starting transfers between devices  45.8 us (18%)
  between operations  22.5 us (9%)
  matrix products  19.5 us (8%)
  local copies, waits for them, and re-layouts  15.3 us (6%)
  other arithmetic  7.41 us (3%)
    all_gather x1, waiting for transfers between devices, on_device(): down_all = lax.all_gather(down_part, 'z', axis=1, tiled=True)  63 us
    ppermute x11, waiting for transfers between devices, turn(): return lax.ppermute(value, axis, [(i, (i + d) % n) for i in range(n)])  54.5 us
    ppermute x11, starting transfers between devices, turn(): return lax.ppermute(value, axis, [(i, (i + d) % n) for i in range(n)])  19.1 us
    ppermute x4, starting transfers between devices, shifted(): lax.ppermute(pack(state), SP, [(i, i + distance) for i in range(length -...  18.8 us
    all_to_all x1, waiting for transfers between devices, on_device(): lax.all_to_all(up_pieces, G, split_axis=0, concat_axis=0, tiled=True)  14.1 us
    dot_general x1, matrix products, on_device(): lifted = jnp.dot(gathered, up_all, preferred_element_type=jnp.float32)  8.92 us
    dot_general x2, matrix products, on_device(): jnp.dot(hidden, down_all[:, k * half:(k + 1) * half], preferred_element_t...  7.12 us
  transfers between devices with their start and end apart: 19, of which 13 were waited for; matrix products, arithmetic and copies ran while one was open for 10% of the time, Pallas kernels for 0%

profile of v2, /device:TPU:0, one launch (start us, length us, event | category | flops | bytes accessed | tf_op | source)
XLA Modules:
  0.0 250.6 jit_solution(453006662361523795)
XLA Ops:
  6.5 2.3 copy.204
  8.9 4.4 %all-to-all-start = ((bf16[4,128,1024]{1,2,0:T(8,128)(2,1)}), bf16[4,128,1024]{1,2,0:T(8,128)(2,1)S(1)}, u32[]{:S(2)}, u32[]{:S(2)}) async-start(bf16[4,128,1024]{1,2,0:T(8,128)(2,1)} %bitcast.1), calls=%async_computation | async-start | bytes 2097152 | tf_op jit(solution)/shard_map/all_to_all | solution.py:97
  13.6 14.1 %all-to-all-done = bf16[4,128,1024]{1,2,0:T(8,128)(2,1)S(1)} async-done(((bf16[4,128,1024]{1,2,0:T(8,128)(2,1)}), bf16[4,128,1024]{1,2,0:T(8,128)(2,1)S(1)}, u32[]{:S(2)}, u32[]{:S(2)}) %all-to-all-start) | async-done | bytes 1048608 | tf_op jit(solution)/shard_map/all_to_all | solution.py:97
  27.7 1.3 copy.205
  29.0 1.2 reduce-window.6
  34.8 1.4 collective-permute-start
  43.2 5.2 %collective-permute-start.1 = (f32[4,72,64]{1,2,0:T(8,128)S(1)}, f32[4,72,64]{1,2,0:T(8,128)S(1)}, u32[]{:S(2)}, u32[]{:S(2)}) collective-permute-start(f32[4,72,64]{1,2,0:T(8,128)S(1)} %maximum_maximum_fusion.1), channel_id=1, source_target_pairs={{0,4},{2,6},{4,8},{6,10},{8,12},{10,14},{12,16},{14,18},{16,20},{1... | collective-permute-start | bytes 221192 | tf_op jit(solution)/shard_map/ppermute | solution.py:55
  48.5 3.6 %collective-permute-done.1 = f32[4,72,64]{1,2,0:T(8,128)S(1)} collective-permute-done((f32[4,72,64]{1,2,0:T(8,128)S(1)}, f32[4,72,64]{1,2,0:T(8,128)S(1)}, u32[]{:S(2)}, u32[]{:S(2)}) %collective-permute-start.1) | collective-permute-done | bytes 73760 | tf_op jit(solution)/shard_map/ppermute | solution.py:55
  55.1 9.8 %collective-permute-start.2 = (f32[4,72,64]{1,2,0:T(8,128)S(1)}, f32[4,72,64]{1,2,0:T(8,128)S(1)}, u32[]{:S(2)}, u32[]{:S(2)}) collective-permute-start(f32[4,72,64]{1,2,0:T(8,128)S(1)} %maximum_maximum_fusion.2), channel_id=1, source_target_pairs={{0,8},{2,10},{4,12},{6,14},{8,16},{10,18},{12,20},{14,22},{16,24},... | collective-permute-start | bytes 221192 | tf_op jit(solution)/shard_map/ppermute | solution.py:55
  65.3 1.6 collective-permute-start.5
  66.9 3.5 %all-to-all-start.1 = ((bf16[4,1024,128]{2,1,0:T(8,128)(2,1)}), bf16[4,1024,128]{2,1,0:T(8,128)(2,1)S(1)}, u32[]{:S(2)}, u32[]{:S(2)}) async-start(bf16[4,1024,128]{2,1,0:T(8,128)(2,1)} %bitcast.33), calls=%async_computation.1 | async-start | bytes 2097152 | tf_op jit(solution)/shard_map/all_to_all | solution.py:104
  73.4 2.3 collective-permute-start.3
  80.4 4.4 %all-to-all-done.1 = bf16[4,1024,128]{2,1,0:T(8,128)(2,1)S(1)} async-done(((bf16[4,1024,128]{2,1,0:T(8,128)(2,1)}), bf16[4,1024,128]{2,1,0:T(8,128)(2,1)S(1)}, u32[]{:S(2)}, u32[]{:S(2)}) %all-to-all-start.1) | async-done | bytes 1048608 | tf_op jit(solution)/shard_map/all_to_all | solution.py:104
  84.8 1.4 copy.223
  86.2 1.8 multiply_reduce_fusion
  88.8 10.8 %collective-permute-done.6 = bf16[128,2048]{1,0:T(8,128)(2,1)S(1)} collective-permute-done((bf16[128,2048]{1,0:T(8,128)(2,1)S(1)}, bf16[128,2048]{1,0:T(8,128)(2,1)S(1)}, u32[]{:S(2)}, u32[]{:S(2)}) %collective-permute-start.6) | collective-permute-done | bytes 524320 | tf_op jit(solution)/shard_map/ppermute | solution.py:61
  99.6 10.0 %collective-permute-start.7 = (bf16[256,2048]{1,0:T(8,128)(2,1)S(1)}, bf16[256,2048]{1,0:T(8,128)(2,1)S(1)}, u32[]{:S(2)}, u32[]{:S(2)}) collective-permute-start(bf16[256,2048]{1,0:T(8,128)(2,1)S(1)} %pad_maximum_fusion.1), channel_id=1, source_target_pairs={{0,4},{4,0},{1,5},{5,1},{2,6},{6,2},{3,7},{7,3},{8,12},{12,8},{9,1... | collective-permute-start | bytes 3145736 | tf_op jit(solution)/shard_map/ppermute | solution.py:61
  109.6 22.2 %collective-permute-done.7 = bf16[256,2048]{1,0:T(8,128)(2,1)S(1)} collective-permute-done((bf16[256,2048]{1,0:T(8,128)(2,1)S(1)}, bf16[256,2048]{1,0:T(8,128)(2,1)S(1)}, u32[]{:S(2)}, u32[]{:S(2)}) %collective-permute-start.7) | collective-permute-done | bytes 1048608 | tf_op jit(solution)/shard_map/ppermute | solution.py:61
  132.0 4.3 %collective-permute-done.8 = bf16[512,2048]{1,0:T(8,128)(2,1)} collective-permute-done((bf16[512,2048]{1,0:T(8,128)(2,1)S(1)}, bf16[512,2048]{1,0:T(8,128)(2,1)}, u32[]{:S(2)}, u32[]{:S(2)}) %collective-permute-start.8) | collective-permute-done | bytes 2097184 | tf_op jit(solution)/shard_map/ppermute | solution.py:61
  136.3 8.9 %multiply_convert_fusion = bf16[1024,1024]{1,0:T(8,128)(2,1)} fusion(bf16[2048,1024]{1,0:T(8,128)(2,1)} %all-gather.3.cloned.1.call-done, bf16[512,2048]{1,0:T(8,128)(2,1)} %collective-permute-done.8, bf16[256,2048]{1,0:T(8,128)(2,1)S(1)} %collective-permute-done.7, bf16[128,2048]{1,0:T(8,128)(2,1)S(1)} %collective-permute-done.6, ...), kind=kOutput, calls=%fused_computation.8 | convolution fusion | flops 4314890240 | bytes 10485760 | tf_op jit(solution)/shard_map/dot_general | solution.py:199
  145.2 63.0 %all-gather.5.cloned.1.call-done = bf16[1024,2048]{0,1:T(8,128)(2,1)} async-done(((bf16[1024,512]{0,1:T(8,128)(2,1)}), bf16[1024,2048]{0,1:T(8,128)(2,1)}) %all-gather.5.cloned.1.call-update) | async-done | bytes 4194320 | tf_op jit(solution)/shard_map/all_gather | solution.py:106
  208.2 4.7 %fusion.19 = bf16[1024,1024]{1,0:T(8,128)(2,1)S(1)} fusion(bf16[1024,1024]{1,0:T(8,128)(2,1)} %multiply_convert_fusion, bf16[1024,2048]{0,1:T(8,128)(2,1)} %all-gather.5.cloned.1.call-done), kind=kOutput, calls=%fused_computation.22 | convolution fusion | flops 2148532224 | bytes 6291456 | tf_op jit(solution)/shard_map/dot_general | solution.py:205
  213.2 1.9 copy-done.8
  215.1 2.4 fusion.22
  218.3 1.5 collective-permute-start.10
  221.0 1.5 collective-permute-start.13
  222.5 10.2 %collective-permute-done.10 = bf16[2,128,1024]{2,1,0:T(8,128)(2,1)S(1)} collective-permute-done((bf16[2,128,1024]{2,1,0:T(8,128)(2,1)S(1)}, bf16[2,128,1024]{2,1,0:T(8,128)(2,1)S(1)}, u32[]{:S(2)}, u32[]{:S(2)}) %collective-permute-start.10) | collective-permute-done | bytes 524320 | tf_op jit(solution)/shard_map/ppermute | solution.py:61
  232.9 1.5 collective-permute-start.11
  235.2 1.5 collective-permute-start.14
  236.8 4.1 %collective-permute-done.11 = bf16[128,1024]{1,0:T(8,128)(2,1)S(1)} collective-permute-done((bf16[128,1024]{1,0:T(8,128)(2,1)S(1)}, bf16[128,1024]{1,0:T(8,128)(2,1)S(1)}, u32[]{:S(2)}, u32[]{:S(2)}) %collective-permute-start.11) | collective-permute-done | bytes 262176 | tf_op jit(solution)/shard_map/ppermute | solution.py:61
  240.9 1.9 collective-permute-done.14
  242.8 0.9 add_convert_fusion
  (140 shorter events, 18.4 us)
Async XLA Ops:
  6.5 6.7 %copy-start.1 = (bf16[256,256]{1,0:T(8,128)(2,1)S(1)}, bf16[256,256]{1,0:T(8,128)(2,1)}, u32[]{:S(2)}) copy-start(bf16[256,256]{1,0:T(8,128)(2,1)} %param.14) | copy-start | bytes 393220
  6.5 6.8 %copy-start.2 = (bf16[256,256]{1,0:T(8,128)(2,1)S(1)}, bf16[256,256]{1,0:T(8,128)(2,1)}, u32[]{:S(2)}) copy-start(bf16[256,256]{1,0:T(8,128)(2,1)} %param.12) | copy-start | bytes 393220
  6.5 6.9 %copy-start.6 = (bf16[2048]{0:T(1024)(128)(2,1)S(1)}, bf16[2048]{0:T(1024)(128)(2,1)}, u32[]{:S(2)}) copy-start(bf16[2048]{0:T(1024)(128)(2,1)} %param.19) | copy-start | bytes 12292
  8.9 20.1 %copy-start.7 = (f32[4,256]{1,0:T(4,128)S(1)}, f32[4,256]{1,0:T(4,128)}, u32[]{:S(2)}) copy-start(f32[4,256]{1,0:T(4,128)} %param.16) | copy-start | bytes 12292
  8.9 22.0 %copy-start.5 = (s32[256]{0:T(256)S(1)}, s32[256]{0:T(256)}, u32[]{:S(2)}) copy-start(s32[256]{0:T(256)} %param.17) | copy-start | bytes 3076
  8.9 23.9 %copy-start.4 = (f32[4,256]{1,0:T(4,128)S(1)}, f32[4,256]{1,0:T(4,128)}, u32[]{:S(2)}) copy-start(f32[4,256]{1,0:T(4,128)} %param.15) | copy-start | bytes 12292
  8.9 24.2 %copy-start.3 = (bf16[256,256]{1,0:T(8,128)(2,1)S(1)}, bf16[256,256]{1,0:T(8,128)(2,1)}, u32[]{:S(2)}) copy-start(bf16[256,256]{1,0:T(8,128)(2,1)} %param.13) | copy-start | bytes 393220
  8.9 18.8 %all-to-all-start = ((bf16[4,128,1024]{1,2,0:T(8,128)(2,1)}), bf16[4,128,1024]{1,2,0:T(8,128)(2,1)S(1)}, u32[]{:S(2)}, u32[]{:S(2)}) async-start(bf16[4,128,1024]{1,2,0:T(8,128)(2,1)} %bitcast.1), calls=%async_computation | async-start | bytes 2097152 | tf_op jit(solution)/shard_map/all_to_all | solution.py:97
  13.3 123.0 %all-gather.3.cloned.1.call-start = ((), (), s32[]{:S(2)}) async-start(), calls=%async_computation.2 | async-start | bytes 5242880 | tf_op jit(solution)/shard_map/all_gather | solution.py:105
  34.7 30.6 %copy-start = (bf16[256,2048]{1,0:T(8,128)(2,1)S(1)}, bf16[256,2048]{1,0:T(8,128)(2,1)}, u32[]{:S(2)}) copy-start(bf16[256,2048]{1,0:T(8,128)(2,1)} %param.18) | copy-start | bytes 3145732
  34.8 3.5 %collective-permute-start = (f32[4,72,64]{1,2,0:T(8,128)S(1)}, f32[4,72,64]{1,2,0:T(8,128)S(1)}, u32[]{:S(2)}, u32[]{:S(2)}) collective-permute-start(f32[4,72,64]{1,2,0:T(8,128)S(1)} %maximum_maximum_fusion), channel_id=1, source_target_pairs={{0,2},{2,4},{4,6},{6,8},{8,10},{10,12},{12,14},{14,16},{16,18},{18... | collective-permute-start | bytes 221192 | tf_op jit(solution)/shard_map/ppermute | solution.py:55
  43.2 8.9 %collective-permute-start.1 = (f32[4,72,64]{1,2,0:T(8,128)S(1)}, f32[4,72,64]{1,2,0:T(8,128)S(1)}, u32[]{:S(2)}, u32[]{:S(2)}) collective-permute-start(f32[4,72,64]{1,2,0:T(8,128)S(1)} %maximum_maximum_fusion.1), channel_id=1, source_target_pairs={{0,4},{2,6},{4,8},{6,10},{8,12},{10,14},{12,16},{14,18},{16,20},{1... | collective-permute-start | bytes 221192 | tf_op jit(solution)/shard_map/ppermute | solution.py:55
  55.1 15.4 %collective-permute-start.2 = (f32[4,72,64]{1,2,0:T(8,128)S(1)}, f32[4,72,64]{1,2,0:T(8,128)S(1)}, u32[]{:S(2)}, u32[]{:S(2)}) collective-permute-start(f32[4,72,64]{1,2,0:T(8,128)S(1)} %maximum_maximum_fusion.2), channel_id=1, source_target_pairs={{0,8},{2,10},{4,12},{6,14},{8,16},{10,18},{12,20},{14,22},{16,24},... | collective-permute-start | bytes 221192 | tf_op jit(solution)/shard_map/ppermute | solution.py:55
  65.3 20.9 %collective-permute-start.5 = (bf16[256,2048]{1,0:T(8,128)(2,1)S(1)}, bf16[256,2048]{1,0:T(8,128)(2,1)}, u32[]{:S(2)}, u32[]{:S(2)}) collective-permute-start(bf16[256,2048]{1,0:T(8,128)(2,1)S(1)} %copy-done), channel_id=1, source_target_pairs={{0,1},{1,0},{2,3},{3,2},{4,5},{5,4},{6,7},{7,6},{8,9},{9,8},{10,11... | collective-permute-start | bytes 3145736 | tf_op jit(solution)/shard_map/ppermute | solution.py:61
  66.9 17.9 %all-to-all-start.1 = ((bf16[4,1024,128]{2,1,0:T(8,128)(2,1)}), bf16[4,1024,128]{2,1,0:T(8,128)(2,1)S(1)}, u32[]{:S(2)}, u32[]{:S(2)}) async-start(bf16[4,1024,128]{2,1,0:T(8,128)(2,1)} %bitcast.33), calls=%async_computation.1 | async-start | bytes 2097152 | tf_op jit(solution)/shard_map/all_to_all | solution.py:104
  70.4 137.8 %all-gather.5.cloned.1.call-start = ((), (), s32[]{:S(2)}) async-start(), calls=%async_computation.3 | async-start | bytes 5242880 | tf_op jit(solution)/shard_map/all_gather | solution.py:106
  73.4 3.3 %collective-permute-start.3 = (f32[4,72,64]{1,2,0:T(8,128)S(1)}, f32[4,72,64]{1,2,0:T(8,128)S(1)}, u32[]{:S(2)}, u32[]{:S(2)}) collective-permute-start(f32[4,72,64]{1,2,0:T(8,128)S(1)} %maximum_maximum_fusion.3), channel_id=1, source_target_pairs={{0,2},{2,4},{4,6},{6,8},{8,10},{10,12},{12,14},{14,16},{16,18},{18... | collective-permute-start | bytes 221192 | tf_op jit(solution)/shard_map/ppermute | solution.py:55
  79.5 6.7 %collective-permute-start.4 = (bf16[128,256]{1,0:T(8,128)(2,1)S(1)}, bf16[128,256]{1,0:T(8,128)(2,1)S(1)}, u32[]{:S(2)}, u32[]{:S(2)}) collective-permute-start(bf16[128,256]{1,0:T(8,128)(2,1)S(1)} %bitcast.131), channel_id=1, source_target_pairs={{0,1},{1,0},{2,3},{3,2},{4,5},{5,4},{6,7},{7,6},{8,9},{9,8},{10,11... | collective-permute-start | bytes 196616 | tf_op jit(solution)/shard_map/ppermute | solution.py:61
  88.2 11.4 %collective-permute-start.6 = (bf16[128,2048]{1,0:T(8,128)(2,1)S(1)}, bf16[128,2048]{1,0:T(8,128)(2,1)S(1)}, u32[]{:S(2)}, u32[]{:S(2)}) collective-permute-start(bf16[128,2048]{1,0:T(8,128)(2,1)S(1)} %multiply_convert_fusion.1), channel_id=1, source_target_pairs={{0,1},{1,0},{2,3},{3,2},{4,5},{5,4},{6,7},{7,6},{8,9},{9,8},{10,11... | collective-permute-start | bytes 1572872 | tf_op jit(solution)/shard_map/ppermute | solution.py:61
  99.6 32.2 %collective-permute-start.7 = (bf16[256,2048]{1,0:T(8,128)(2,1)S(1)}, bf16[256,2048]{1,0:T(8,128)(2,1)S(1)}, u32[]{:S(2)}, u32[]{:S(2)}) collective-permute-start(bf16[256,2048]{1,0:T(8,128)(2,1)S(1)} %pad_maximum_fusion.1), channel_id=1, source_target_pairs={{0,4},{4,0},{1,5},{5,1},{2,6},{6,2},{3,7},{7,3},{8,12},{12,8},{9,1... | collective-permute-start | bytes 3145736 | tf_op jit(solution)/shard_map/ppermute | solution.py:61
  131.9 4.4 %collective-permute-start.8 = (bf16[512,2048]{1,0:T(8,128)(2,1)S(1)}, bf16[512,2048]{1,0:T(8,128)(2,1)}, u32[]{:S(2)}, u32[]{:S(2)}) collective-permute-start(bf16[512,2048]{1,0:T(8,128)(2,1)S(1)} %pad_maximum_fusion), channel_id=1, source_target_pairs={{0,2},{2,0},{1,3},{3,1},{4,6},{6,4},{5,7},{7,5},{8,10},{10,8},{9,1... | collective-permute-start | bytes 6291464 | tf_op jit(solution)/shard_map/ppermute | solution.py:61
  208.2 5.0 %copy-start.9 = (bf16[1024,1024]{1,0:T(8,128)(2,1)S(1)}, bf16[1024,1024]{1,0:T(8,128)(2,1)}, u32[]{:S(2)}) copy-start(bf16[1024,1024]{1,0:T(8,128)(2,1)} %multiply_convert_fusion) | copy-start | bytes 6291460
  212.9 2.2 copy-start.8
  213.1 4.7 %collective-permute-start.9 = (bf16[2,2,128,1024]{3,2,1,0:T(8,128)(2,1)S(1)}, bf16[2,2,128,1024]{3,2,1,0:T(8,128)(2,1)S(1)}, u32[]{:S(2)}, u32[]{:S(2)}) collective-permute-start(bf16[2,2,128,1024]{3,2,1,0:T(8,128)(2,1)S(1)} %bitcast.126), channel_id=1, source_target_pairs={{0,2},{2,0},{1,3},{3,1},{4,6},{6,4},{5,7},{7,5},{8,10},{10,8},{9,1... | collective-permute-start | bytes 3145736 | tf_op jit(solution)/shard_map/ppermute | solution.py:61
  217.8 2.7 %collective-permute-start.12 = (bf16[2,2,128,1024]{3,2,0,1:T(8,128)(2,1)S(1)}, bf16[2,2,128,1024]{3,2,0,1:T(8,128)(2,1)S(1)}, u32[]{:S(2)}, u32[]{:S(2)}) collective-permute-start(bf16[2,2,128,1024]{3,2,0,1:T(8,128)(2,1)S(1)} %copy.224), channel_id=1, source_target_pairs={{0,2},{2,0},{1,3},{3,1},{4,6},{6,4},{5,7},{7,5},{8,10},{10,8},{9,1... | collective-permute-start | bytes 3145736 | tf_op jit(solution)/shard_map/ppermute | solution.py:61
  218.3 14.4 %collective-permute-start.10 = (bf16[2,128,1024]{2,1,0:T(8,128)(2,1)S(1)}, bf16[2,128,1024]{2,1,0:T(8,128)(2,1)S(1)}, u32[]{:S(2)}, u32[]{:S(2)}) collective-permute-start(bf16[2,128,1024]{2,1,0:T(8,128)(2,1)S(1)} %slice_bitcast_fusion.2), channel_id=1, source_target_pairs={{0,4},{4,0},{1,5},{5,1},{2,6},{6,2},{3,7},{7,3},{8,12},{12,8},{9,1... | collective-permute-start | bytes 1572872 | tf_op jit(solution)/shard_map/ppermute | solution.py:61
  221.0 14.0 %collective-permute-start.13 = (bf16[2,128,1024]{2,1,0:T(8,128)(2,1)S(1)}, bf16[2,128,1024]{2,1,0:T(8,128)(2,1)S(1)}, u32[]{:S(2)}, u32[]{:S(2)}) collective-permute-start(bf16[2,128,1024]{2,1,0:T(8,128)(2,1)S(1)} %slice_bitcast_fusion), channel_id=1, source_target_pairs={{0,1},{1,0},{2,3},{3,2},{4,5},{5,4},{6,7},{7,6},{8,9},{9,8},{10,11... | collective-permute-start | bytes 1572872 | tf_op jit(solution)/shard_map/ppermute | solution.py:61
  232.9 7.9 %collective-permute-start.11 = (bf16[128,1024]{1,0:T(8,128)(2,1)S(1)}, bf16[128,1024]{1,0:T(8,128)(2,1)S(1)}, u32[]{:S(2)}, u32[]{:S(2)}) collective-permute-start(bf16[128,1024]{1,0:T(8,128)(2,1)S(1)} %slice_bitcast_fusion.6), channel_id=1, source_target_pairs={{0,1},{1,0},{2,3},{3,2},{4,5},{5,4},{6,7},{7,6},{8,9},{9,8},{10,11... | collective-permute-start | bytes 786440 | tf_op jit(solution)/shard_map/ppermute | solution.py:61
  235.2 7.6 %collective-permute-start.14 = (bf16[128,1024]{1,0:T(8,128)(2,1)S(1)}, bf16[128,1024]{1,0:T(8,128)(2,1)S(1)}, u32[]{:S(2)}, u32[]{:S(2)}) collective-permute-start(bf16[128,1024]{1,0:T(8,128)(2,1)S(1)} %slice_bitcast_fusion.4), channel_id=1, source_target_pairs={{0,4},{4,0},{1,5},{5,1},{2,6},{6,2},{3,7},{7,3},{8,12},{12,8},{9,1... | collective-permute-start | bytes 786440 | tf_op jit(solution)/shard_map/ppermute | solution.py:61
Sparse Core Ops, SparseCore 0:
  38.5 83.6 all-gather.2
  123.7 84.4 all-gather.4
